TPU v7x, 32 devices: a whole 2x2x4 slice. The times are simulated.
32 devices in a mesh: ep: 8 (over z, y), tp: 4 (over x, core).
Axes of the slice: x: 2, y: 2, z: 4, core: 2. Of those that a mesh axis runs over, the one named last changes fastest.
Arguments:
- conv_value: bfloat16 [4096, 2048], P('ep', 'tp'), may hold values from -6 to 6
- conv_gate: bfloat16 [4096, 2048], P('ep', 'tp'), may hold values from -9 to 9
- conv_kernel: float32 [31, 2048], P(None, 'tp'), may hold values from -20 to 20
- norm_gain: float32 [2048], P('tp'), may hold values from 0.1 to 1.9
- mixer_proj: bfloat16 [2048, 2048], P('tp'), may hold values from -0.125 to 0.125
- moe_in: bfloat16 [4096, 2048], P('ep'), may hold values from -6 to 6
- route_ids: int32 [4096, 2], P('ep'), may hold values from 0 to 7, all different within a row; in each aligned block of 128 rows (0 to 127, 128 to 255, ...) at most 64 rows name the same one
- route_logits: float32 [4096, 2], P('ep'), may hold values from -6 to 6
- moe_gain: float32 [2048], replicated, may hold values from 0.1 to 1.9
- expert_gate: bfloat16 [8, 2048, 2048], P('ep', None, 'tp'), may hold values from -0.26367188 to 0.26367188
- expert_lin: bfloat16 [8, 2048, 2048], P('ep', None, 'tp'), may hold values from -0.26367188 to 0.26367188
- expert_down: bfloat16 [8, 2048, 2048], P('ep', 'tp'), may hold values from -0.052978516 to 0.052978516
Outputs:
- mixer_out: bfloat16 [4096, 2048], P(('ep', 'tp'))
- moe_out: bfloat16 [4096, 2048], P(('ep', 'tp'))
Inputs may be any that keep to these rules, and one draw needn't show every extreme that they name: `route_ids`: every row names 2 different experts. In each aligned block of 128 rows (one device's output rows) no expert is named by more than 64 rows, and in every draw some expert is named by exactly 64 rows of some block.
All inputs are finite; a program needn't handle non-finite values.
Results may differ from a plain program's by a relative error of at most 0.01.
Values may be sent and summed in bfloat16 or wider, within the bound.
A program may use at most 128 MiB of HBM per device.

v0:
```python
import jax
import jax.numpy as jnp
from jax import lax
from jax.sharding import PartitionSpec as P

EPS = 1e-05
LIMIT = 7.0
SLOPE = 1.702


def passed_along(block, axis, distance):
    devices = range(lax.axis_size(axis))
    route = [(i - distance, i) for i in devices if i - distance in devices]
    return lax.ppermute(block, axis, route)


def slot_targets(routes, experts, capacity):
    flat = routes.reshape(-1)
    onehot = (flat[:, None] == jnp.arange(experts, dtype=jnp.int32)[None, :]).astype(jnp.int32)
    rank = jnp.sum(jnp.cumsum(onehot, axis=0) * onehot, axis=1) - 1
    return flat * capacity + rank


def slot_sources(target, total, topk):
    hits = (target[None, :] == jnp.arange(total, dtype=jnp.int32)[:, None]).astype(jnp.int32)
    owner = jnp.arange(target.shape[0], dtype=jnp.int32) // topk
    source = jnp.sum(hits * owner[None, :], axis=1)
    filled = jnp.sum(hits, axis=1) > 0
    return (source, filled)


def shards(
    conv_value,
    conv_gate,
    conv_kernel,
    norm_gain,
    mixer_proj,
    moe_in,
    route_ids,
    route_logits,
    moe_gain,
    expert_gate,
    expert_lin,
    expert_down,
):
    tp_size = lax.axis_size("tp")
    tp_index = lax.axis_index("tp")
    glu = (conv_value.astype(jnp.float32) * jax.nn.sigmoid(conv_gate.astype(jnp.float32))).astype(
        jnp.bfloat16
    )
    reach = conv_kernel.shape[0] - 1
    length = glu.shape[0]
    rim = passed_along(glu[length - reach :], "ep", 1)
    padded = jnp.concatenate([rim, glu], axis=0).astype(jnp.float32)
    conv = jnp.zeros(glu.shape, jnp.float32)
    for tap in range(reach + 1):
        conv = conv + conv_kernel[tap][None, :] * padded[tap : tap + length]
    total, square = lax.psum((jnp.sum(conv, axis=1), jnp.sum(conv * conv, axis=1)), "tp")
    channels = conv.shape[1] * tp_size
    mean = (total / channels)[:, None]
    var = (square / channels)[:, None] - mean * mean
    conv_act = jax.nn.silu((conv - mean) * lax.rsqrt(var + EPS) * norm_gain).astype(jnp.bfloat16)
    piece = conv_act
    mixer_out = lax.psum_scatter(
        jnp.dot(piece, mixer_proj, preferred_element_type=jnp.float32).astype(jnp.bfloat16),
        "tp",
        scatter_dimension=0,
        tiled=True,
    )
    rows = moe_in.shape[0] // tp_size
    topk = route_ids.shape[1]
    experts = lax.axis_size("ep")
    capacity = max(2, 2 * rows * topk // experts)
    width = moe_in.shape[1]
    start = tp_index * rows
    block = lax.dynamic_slice_in_dim(moe_in, start, rows, 0).astype(jnp.float32)
    mu = jnp.mean(block, axis=1, keepdims=True)
    va = jnp.mean(jnp.square(block - mu), axis=1, keepdims=True)
    normed = ((block - mu) * lax.rsqrt(va + EPS) * moe_gain).astype(jnp.bfloat16)
    routes = lax.dynamic_slice_in_dim(route_ids, start, rows, 0)
    target = slot_targets(routes, experts, capacity)
    source, filled = slot_sources(target, experts * capacity, topk)
    packed = jnp.where(filled[:, None], normed[source], jnp.zeros((), jnp.bfloat16))
    packed, own_target = (packed.reshape(experts, capacity, width), target)
    landed = lax.all_to_all(packed[None], "ep", split_axis=1, concat_axis=1, tiled=True)
    arrived = lax.all_gather(landed, "tp", axis=0, tiled=True)
    flat = arrived.reshape(-1, width)
    piece = flat
    gate = jnp.minimum(jnp.dot(piece, expert_gate[0], preferred_element_type=jnp.float32), LIMIT)
    lin = jnp.clip(jnp.dot(piece, expert_lin[0], preferred_element_type=jnp.float32), -LIMIT, LIMIT)
    hidden = (gate * jax.nn.sigmoid(SLOPE * gate) * (lin + 1.0)).astype(jnp.bfloat16)
    results = lax.psum_scatter(
        jnp.dot(hidden, expert_down[0], preferred_element_type=jnp.float32).astype(jnp.bfloat16),
        "tp",
        scatter_dimension=0,
        tiled=True,
    )
    returned = lax.all_to_all(
        results.reshape(experts, capacity, width), "ep", split_axis=0, concat_axis=0, tiled=True
    )
    picked = (
        returned.reshape(experts * capacity, width)[own_target]
        .astype(jnp.float32)
        .reshape(rows, topk, width)
    )
    logits = lax.dynamic_slice_in_dim(route_logits, tp_index * rows, rows, 0)
    expo = jnp.exp(logits)
    weight = expo / jnp.sum(expo, axis=1, keepdims=True)
    moe_out = jnp.sum(picked * weight[:, :, None], axis=1).astype(jnp.bfloat16)
    return (mixer_out, moe_out)


def solution(mesh):
    placed = (
        P("ep", "tp"),
        P("ep", "tp"),
        P(None, "tp"),
        P("tp"),
        P("tp", None),
        P("ep", None),
        P("ep", None),
        P("ep", None),
        P(),
        P("ep", None, "tp"),
        P("ep", None, "tp"),
        P("ep", "tp", None),
    )
    return jax.shard_map(
        shards,
        mesh=mesh,
        in_specs=placed,
        out_specs=(P(("ep", "tp"), None), P(("ep", "tp"), None)),
        check_vma=False,
    )
```

profile of v0, /device:TPU:0, one launch (start us, length us, event | category | flops | bytes accessed | tf_op | source)
XLA Modules:
  0.0 296.1 jit_solution(3399808234655824898)
XLA Ops:
  7.2 0.0 copy-start
  7.2 0.0 all-gather.2.cloned.1.call-start
  7.2 0.8 broadcast_multiply_fusion.1
  8.1 0.1 copy.25
  8.2 0.1 eq.39
  8.3 0.1 reshape.150
  8.5 0.6 reduce-window.6
  9.0 0.2 slice_reduce_fusion
  9.3 0.1 fusion.43
  9.4 0.3 convert_reduce_fusion.1
  9.7 1.2 convert_reduce_fusion
  10.9 1.3 fusion.6
  12.2 0.1 gt.11
  12.3 1.4 fusion.8
  13.8 3.3 %gather_fusion = bf16[512,2048]{1,0:T(8,128)(2,1)} fusion(bf16[128,2048]{1,0:T(8,128)(2,1)S(1)} %fusion.8, s32[1024]{0:T(1024)S(1)} %pad_clamp_fusion.1), kind=kCustom, calls=%fused_computation | custom fusion | bytes 4196352 | tf_op jit(solution)/shard_map/gather | solution.py:83
  17.1 1.8 broadcast_select_fusion
  18.9 55.4 %all_to_all.10 = bf16[1,8,64,2048]{3,2,0,1:T(8,128)(2,1)} all-to-all(bf16[1,8,64,2048]{3,2,0,1:T(8,128)(2,1)S(1)} %broadcast_select_fusion), channel_id=1, replica_groups=mesh['ep'=8,'tp'=4] {'ep'}, dimensions={1} | all-to-all | bytes 4194304 | tf_op jit(solution)/shard_map/all_to_all | solution.py:85
  74.4 0.0 all-gather.2.cloned.1.call-update
  74.4 0.0 reduce-scatter.5.cloned.1.call-start
  74.4 57.4 %all-gather.2.cloned.1.call-done = bf16[4,8,64,2048]{3,2,1,0:T(8,128)(2,1)} async-done(((bf16[1,8,64,2048]{3,2,1,0:T(8,128)(2,1)}), bf16[4,8,64,2048]{3,2,1,0:T(8,128)(2,1)}) %all-gather.2.cloned.1.call-update) | async-done | bytes 8388624 | tf_op jit(solution)/shard_map/all_gather | solution.py:86
  131.8 0.0 copy-start.5
  131.8 0.0 copy-start.6
  131.8 7.7 %fusion.2 = f32[2048,512]{1,0:T(8,128)S(1)} fusion(bf16[2048,2048]{1,0:T(8,128)(2,1)} %bitcast.99, bf16[1,2048,512]{2,1,0:T(8,128)(2,1)} %param.21), kind=kOutput, calls=%fused_computation.7 | convolution fusion | flops 4294967296 | bytes 14680064 | tf_op jit(solution)/shard_map/dot_general | solution.py:89
  139.5 0.0 copy-done.5
  139.5 0.0 copy-done.6
  139.5 5.6 %multiply_convert_fusion = bf16[2048,512]{1,0:T(8,128)(2,1)S(1)} fusion(f32[2048,512]{1,0:T(8,128)S(1)} %fusion.2, bf16[2048,2048]{1,0:T(8,128)(2,1)S(1)} %bitcast.100, bf16[1,2048,512]{2,1,0:T(8,128)(2,1)S(1)} %copy-done.6), kind=kOutput, calls=%fused_computation.3 | convolution fusion | flops 4305453056 | bytes 16777216 | tf_op jit(solution)/shard_map/dot_general | solution.py:90
  145.1 0.0 copy-done
  145.1 6.8 %convolution_convert_fusion = bf16[2048,2048]{1,0:T(8,128)(2,1)} fusion(bf16[2048,512]{1,0:T(8,128)(2,1)S(1)} %multiply_convert_fusion, bf16[1,512,2048]{2,1,0:T(8,128)(2,1)S(1)} %copy-done), kind=kOutput, calls=%fused_computation.2 | convolution fusion | flops 4299161600 | bytes 12582912 | tf_op jit(solution)/shard_map/dot_general | solution.py:93
  151.9 0.0 copy-start.1
  151.9 0.0 copy-start.2
  151.9 0.0 copy-start.3
  151.9 0.0 reduce-scatter.5.cloned.1.call-update
  152.0 0.0 reduce-scatter.3.cloned.1.call-start
  152.0 1.0 copy-done.1
  153.0 0.2 copy-done.2
  153.1 0.3 multiply_convert_fusion.2
  153.4 3.4 %collective-permute-start = (bf16[30,512]{1,0:T(8,128)(2,1)S(1)}, bf16[30,512]{1,0:T(8,128)(2,1)S(1)}, u32[]{:S(2)}, u32[]{:S(2)}) collective-permute-start(bf16[30,512]{1,0:T(8,128)(2,1)S(1)} %slice.264), channel_id=1, source_target_pairs={{0,4},{4,8},{8,12},{12,16},{16,20},{20,24},{24,28},{1,5},{5,9},{9,... | collective-permute-start | bytes 92168 | tf_op jit(solution)/shard_map/ppermute | solution.py:14
  156.8 0.0 copy-done.3
  156.9 1.5 collective-permute-done
  158.4 0.2 maximum_convert_fusion
  158.6 0.0 copy-start.7
  158.6 5.0 %fusion.47 = (f32[512]{0:T(512)S(1)}, f32[512]{0:T(512)S(1)}, f32[512,512]{1,0:T(8,128)S(1)}) fusion(f32[542,512]{1,0:T(8,128)S(1)} %maximum_convert_fusion, f32[512]{0:T(512)S(1)} %bitcast.93, f32[512]{0:T(512)S(1)} %bitcast.94, f32[512]{0:T(512)S(1)} %bitcast.65, f32[512]{0:T(512)S(1)} %bitcast.66, f32[512]{0:T(512)S(1)} %bitcast.67, f32[512]{0:T(512)S(1)} %bitcast.68, ...), kind=kLoop, calls=%fused_computation.117 | loop fusion | flops 16776192 | bytes 33622016 | tf_op jit(solution)/shard_map/reduce_sum | solution.py:58
  163.6 6.1 %all-reduce = (f32[512]{0:T(512)S(1)}, f32[512]{0:T(512)S(1)}) all-reduce(f32[512]{0:T(512)S(1)} %get-tuple-element.3, f32[512]{0:T(512)S(1)} %get-tuple-element.2), channel_id=1, replica_groups=mesh['ep'=8,'tp'=4] {'tp'}, use_global_device_ids=true, to_apply=%region_3.0 | all-reduce | flops 1024 | bytes 8192 | tf_op jit(solution)/shard_map/psum | solution.py:58
  169.8 0.0 copy-done.7
  169.8 4.4 %convolution_convert_fusion.1 = bf16[512,2048]{1,0:T(8,128)(2,1)} fusion(bf16[512,2048]{1,0:T(8,128)(2,1)} %param.16, f32[512,512]{1,0:T(8,128)S(1)} %get-tuple-element.10, f32[512]{0:T(512)S(1)} %copy-done.7, f32[512]{0:T(512)S(1)} %get-tuple-element.43, f32[512]{0:T(512)S(1)} %get-tuple-element.42), kind=kOutput, calls=%fused_computation.4 | convolution fusion | flops 1076887552 | bytes 5249024 | tf_op jit(solution)/shard_map/dot_general | solution.py:65
  174.2 0.0 reduce-scatter.3.cloned.1.call-update
  174.2 49.3 %reduce-scatter.5.cloned.1.call-done = bf16[512,2048]{1,0:T(8,128)(2,1)} async-done(((bf16[2048,2048]{1,0:T(8,128)(2,1)}), bf16[512,2048]{1,0:T(8,128)(2,1)}) %reduce-scatter.5.cloned.1.call-update) | async-done | bytes 2097168 | tf_op jit(solution)/shard_map/reduce_scatter | solution.py:92
  223.5 0.0 copy-start.4
  223.5 5.6 %all-to-all-start.1 = ((bf16[8,64,2048]{2,1,0:T(8,128)(2,1)}), bf16[8,64,2048]{2,1,0:T(8,128)(2,1)}, u32[]{:S(2)}, u32[]{:S(2)}) async-start(bf16[8,64,2048]{2,1,0:T(8,128)(2,1)} %bitcast.63), calls=%async_computation.3 | async-start | bytes 4194304 | tf_op jit(solution)/shard_map/all_to_all | solution.py:98
  229.2 0.1 copy.29
  229.3 0.1 mul.532
  229.4 0.0 copy-done.4
  229.5 0.1 copy.30
  229.6 47.7 %all-to-all-done.1 = bf16[8,64,2048]{2,1,0:T(8,128)(2,1)} async-done(((bf16[8,64,2048]{2,1,0:T(8,128)(2,1)}), bf16[8,64,2048]{2,1,0:T(8,128)(2,1)}, u32[]{:S(2)}, u32[]{:S(2)}) %all-to-all-start.1) | async-done | bytes 2097184 | tf_op jit(solution)/shard_map/all_to_all | solution.py:98
  277.4 4.2 %gather_fusion.1 = bf16[256,2048]{1,0:T(8,128)(2,1)S(1)} fusion(bf16[512,2048]{1,0:T(8,128)(2,1)} %bitcast.43, s32[1024]{0:T(1024)S(1)} %pad_clamp_fusion), kind=kCustom, calls=%fused_computation.1 | custom fusion | bytes 2098176 | tf_op jit(solution)/shard_map/gather | solution.py:102
  281.6 2.4 reshape.155
  284.0 5.6 %multiply_reduce_fusion = bf16[128,2048]{1,0:T(8,128)(2,1)} fusion(f32[128,2,2048]{2,1,0:T(2,128)} %reshape.155, f32[128,2]{1,0:T(8,128)S(1)} %copy.30), kind=kLoop, calls=%fused_computation.9 | loop fusion | flops 786432 | bytes 2622464 | tf_op jit(solution)/shard_map/reduce_sum | solution.py:109
  289.5 0.0 reduce-scatter.3.cloned.1.call-done
  (17 shorter events, 0.2 us)
Async XLA Ops:
  7.2 138.0 %copy-start = (bf16[1,512,2048]{2,1,0:T(8,128)(2,1)S(1)}, bf16[1,512,2048]{2,1,0:T(8,128)(2,1)}, u32[]{:S(2)}) copy-start(bf16[1,512,2048]{2,1,0:T(8,128)(2,1)} %param.23) | copy-start | bytes 6291460
  7.2 124.6 %all-gather.2.cloned.1.call-start = ((), (), s32[]{:S(2)}) async-start(), calls=%async_computation.5 | async-start | bytes 10485760 | tf_op jit(solution)/shard_map/all_gather | solution.py:86
  74.4 149.1 %reduce-scatter.5.cloned.1.call-start = ((), (), s32[]{:S(2)}) async-start(), calls=%async_computation.6 | async-start | bytes 10485760 | tf_op jit(solution)/shard_map/reduce_scatter | solution.py:92
  131.8 7.7 %copy-start.5 = (bf16[4,8,64,2048]{3,2,1,0:T(8,128)(2,1)S(1)}, bf16[4,8,64,2048]{3,2,1,0:T(8,128)(2,1)}, u32[]{:S(2)}) copy-start(bf16[4,8,64,2048]{3,2,1,0:T(8,128)(2,1)} %all-gather.2.cloned.1.call-done) | copy-start | bytes 25165828
  131.8 7.7 %copy-start.6 = (bf16[1,2048,512]{2,1,0:T(8,128)(2,1)S(1)}, bf16[1,2048,512]{2,1,0:T(8,128)(2,1)}, u32[]{:S(2)}) copy-start(bf16[1,2048,512]{2,1,0:T(8,128)(2,1)} %param.22) | copy-start | bytes 6291460
  151.9 1.0 copy-start.1
  151.9 1.2 copy-start.2
  151.9 4.9 %copy-start.3 = (f32[31,512]{1,0:T(8,128)S(1)}, f32[31,512]{1,0:T(8,128)}, u32[]{:S(2)}) copy-start(f32[31,512]{1,0:T(8,128)} %param.14) | copy-start | bytes 190468
  152.0 137.6 %reduce-scatter.3.cloned.1.call-start = ((), (), s32[]{:S(2)}) async-start(), calls=%async_computation.4 | async-start | bytes 2621440 | tf_op jit(solution)/shard_map/reduce_scatter | solution.py:64
  153.4 5.0 %collective-permute-start = (bf16[30,512]{1,0:T(8,128)(2,1)S(1)}, bf16[30,512]{1,0:T(8,128)(2,1)S(1)}, u32[]{:S(2)}, u32[]{:S(2)}) collective-permute-start(bf16[30,512]{1,0:T(8,128)(2,1)S(1)} %slice.264), channel_id=1, source_target_pairs={{0,4},{4,8},{8,12},{12,16},{16,20},{20,24},{24,28},{1,5},{5,9},{9,... | collective-permute-start | bytes 92168 | tf_op jit(solution)/shard_map/ppermute | solution.py:14
  158.6 11.2 %copy-start.7 = (f32[512]{0:T(512)S(1)}, f32[512]{0:T(512)}, u32[]{:S(2)}) copy-start(f32[512]{0:T(512)} %param.15) | copy-start | bytes 6148
  223.5 5.9 %copy-start.4 = (f32[512,2]{0,1:T(2,128)S(1)}, f32[512,2]{0,1:T(2,128)}, u32[]{:S(2)}) copy-start(f32[512,2]{0,1:T(2,128)} %param.19) | copy-start | bytes 12292
  223.5 53.8 %all-to-all-start.1 = ((bf16[8,64,2048]{2,1,0:T(8,128)(2,1)}), bf16[8,64,2048]{2,1,0:T(8,128)(2,1)}, u32[]{:S(2)}, u32[]{:S(2)}) async-start(bf16[8,64,2048]{2,1,0:T(8,128)(2,1)} %bitcast.63), calls=%async_computation.3 | async-start | bytes 4194304 | tf_op jit(solution)/shard_map/all_to_all | solution.py:98
Sparse Core Ops, SparseCore 0:
  74.5 57.2 all-gather.1
  152.1 71.4 reduce-scatter.4
  226.6 31.1 reduce-scatter.2
where the time goes:
time: 297 us; the launch traced here: 296 us
  waiting for transfers between devices  156 us (53%)
  blocking collectives  61.6 us (21%)
  matrix products  24.5 us (8%)
  other arithmetic  18.7 us (6%)
  between operations  14 us (5%)
  local copies, waits for them, and re-layouts  12.2 us (4%)
  starting transfers between devices  9.16 us (3%)
    all_gather x1, waiting for transfers between devices, shards(): arrived = lax.all_gather(landed, 'tp', axis=0, tiled=True)  57.4 us
    all_to_all x1, blocking collectives, shards(): lax.all_to_all(packed[None], 'ep', split_axis=1, concat_axis=1, tiled=True)  55.4 us
    reduce_scatter x1, waiting for transfers between devices, shards(): lax.psum_scatter(jnp.dot(hidden, expert_down[0], preferred_element_type=j...  49.3 us
    all_to_all x1, waiting for transfers between devices, shards(): lax.all_to_all(results.reshape(experts, capacity, width), 'ep', split_axi...  47.7 us
    dot_general x1, matrix products, shards(): jnp.dot(piece, expert_gate[0], preferred_element_type=jnp.float32)  7.67 us
    dot_general x1, matrix products, shards(): jnp.dot(hidden, expert_down[0], preferred_element_type=jnp.float32)  6.79 us
    psum x1, blocking collectives, shards(): lax.psum((jnp.sum(conv, axis=1), jnp.sum(conv * conv, axis=1)), 'tp')  6.11 us
  transfers between devices with their start and end apart: 5, of which 4 were waited for; matrix products, arithmetic and copies ran while one was open for 8% of the time, Pallas kernels for 0%

commit v1 on v0

v1 whole, which is shorter than its diff:
```python
import jax
import jax.numpy as jnp
from jax import lax
from jax.experimental import pallas as pl
from jax.experimental.pallas import tpu as pltpu
from jax.sharding import PartitionSpec as P

EPS = 1e-05
LIMIT = 7.0
SLOPE = 1.702
F32 = jnp.float32
BF16 = jnp.bfloat16


def passed_along(block, axis, distance):
    devices = range(lax.axis_size(axis))
    route = [(i - distance, i) for i in devices if i - distance in devices]
    return lax.ppermute(block, axis, route)


def slot_targets(routes, experts, capacity):
    flat = routes.reshape(-1)
    onehot = (flat[:, None] == jnp.arange(experts, dtype=jnp.int32)[None, :]).astype(jnp.int32)
    rank = jnp.sum(jnp.cumsum(onehot, axis=0) * onehot, axis=1) - 1
    return flat * capacity + rank


def remote(src, dst, send, recv, device):
    return pltpu.make_async_remote_copy(
        src_ref=src,
        dst_ref=dst,
        send_sem=send,
        recv_sem=recv,
        device_id=device,
        device_id_type=pl.DeviceIdType.MESH,
    )


def joined(block):
    groups, rows, width = block.shape
    if rows % 16:
        return block.astype(F32).reshape(groups * rows, width).astype(BF16)
    return block.reshape(groups * rows, width)


def layer_kernel(
    packed, act, wmat, gate_hbm, lin_hbm, down_hbm, proj_hbm,
    mix_out, moe_out,
    gate_w, lin_w, down_w, proj_w,
    arrived, part, a_recv, b_send, b_recv, c_send, c_recv,
    m_part, m_a, m_bs, m_b,
    load_sem, sems, m_sems,
):
    experts, cap, width = packed.shape
    rows = moe_out.shape[0]
    ep, tp = lax.axis_index("ep"), lax.axis_index("tp")
    core, side = lax.rem(tp, 2), lax.div(tp, 2)
    xpeer, cpeer = {"tp": lax.rem(tp + 2, 4)}, {"tp": tp + 1 - 2 * core}
    pos, posx = core * 2 + side, core * 2 + 1 - side
    posc, posd = (1 - core) * 2 + side, (1 - core) * 2 + 1 - side

    def chunk(d):
        return lax.rem(ep - d + experts, experts)

    def prim(d):
        e = lax.rem(ep + d, experts)
        return remote(packed.at[e], arrived.at[ep, pos], sems.at[0, d], sems.at[1, d], {"ep": e})

    def prim_in(d):
        slot = arrived.at[chunk(d), pos]
        return remote(slot, slot, sems.at[0, d], sems.at[1, d], {"ep": chunk(d)})

    own = pltpu.make_async_copy(packed.at[ep], arrived.at[ep, pos], load_sem.at[4])

    def hop(d, place, k, peer):
        slot = arrived.at[chunk(d), place]
        return remote(slot, slot, sems.at[k, d], sems.at[k + 1, d], peer)

    def xf(d):
        return hop(d, pos, 2, xpeer)

    def xf_in(d):
        return hop(d, posx, 2, xpeer)

    def cf(d):
        return hop(d, pos, 4, cpeer)

    def cf_in(d):
        return hop(d, posc, 4, cpeer)

    def cf2(d):
        return hop(d, posx, 6, cpeer)

    def cf2_in(d):
        return hop(d, posd, 6, cpeer)

    def give_a(d):
        s = chunk(d)
        return remote(part.at[s, 1 - core], a_recv.at[s], sems.at[8, d], sems.at[9, d], cpeer)

    def give_b(d):
        s = chunk(d)
        return remote(b_send.at[s], b_recv.at[s], sems.at[10, d], sems.at[11, d], xpeer)

    def give_c(d):
        s = chunk(d)
        return remote(c_send.at[s], c_recv.at[ep], sems.at[12, d], sems.at[13, d], {"ep": s})

    def give_c_in(d):
        e = lax.rem(ep + d, experts)
        return remote(c_recv.at[e], c_recv.at[e], sems.at[12, d], sems.at[13, d], {"ep": e})

    mix_a = remote(m_part.at[1 - core], m_a, m_sems.at[0], m_sems.at[1], cpeer)
    mix_b = remote(m_bs, m_b, m_sems.at[2], m_sems.at[3], xpeer)

    own.start()

    @pl.loop(1, experts)
    def _(d):
        prim(d).start()

    loads = [
        pltpu.make_async_copy(proj_hbm, proj_w, load_sem.at[3]),
        pltpu.make_async_copy(gate_hbm, gate_w, load_sem.at[0]),
        pltpu.make_async_copy(lin_hbm, lin_w, load_sem.at[1]),
        pltpu.make_async_copy(down_hbm, down_w, load_sem.at[2]),
    ]
    for load in loads:
        load.start()
    own.wait()
    xf(0).start()
    cf(0).start()

    loads[0].wait()
    for t in range(4):
        m_part[t % 2, t // 2] = jnp.dot(
            act[t * rows : (t + 1) * rows, :], proj_w[...], preferred_element_type=F32
        ).astype(BF16)
    mix_a.start()
    for load in loads[1:]:
        load.wait()

    def ffn(d):
        s = chunk(d)
        x = joined(arrived[s])
        gate = jnp.minimum(jnp.dot(x, gate_w[...], preferred_element_type=F32), LIMIT)
        lin = jnp.clip(jnp.dot(x, lin_w[...], preferred_element_type=F32), -LIMIT, LIMIT)
        hidden = (gate * jax.nn.sigmoid(SLOPE * gate) * (lin + 1.0)).astype(BF16)
        tile = min(512, width)
        for n in range(0, width, tile):
            y = jnp.dot(hidden, down_w[:, n : n + tile], preferred_element_type=F32)
            part[s, :, :, :, n : n + tile] = y.reshape(2, 2, cap, tile).astype(BF16)

    def at_step(i, lag, first=0):
        return jnp.logical_and(i - lag >= first, i - lag < experts)

    @pl.loop(0, experts + 4)
    def _(i):
        @pl.when(at_step(i, 0, 1))
        def _():
            prim_in(i).wait_recv()
            xf(i).start()
            cf(i).start()

        @pl.when(at_step(i, 1))
        def _():
            xf_in(i - 1).wait_recv()
            cf2(i - 1).start()

        @pl.when(at_step(i, 2))
        def _():
            cf_in(i - 2).wait_recv()
            cf2_in(i - 2).wait_recv()
            ffn(i - 2)
            give_a(i - 2).start()

        @pl.when(at_step(i, 3))
        def _():
            d = i - 3
            s = chunk(d)
            give_a(d).wait_recv()
            b_send[s] = (part[s, core, 1 - side].astype(F32) + a_recv[s, 1 - side].astype(F32)).astype(BF16)
            give_b(d).start()

        @pl.when(i == 3)
        def _():
            mix_a.wait_recv()
            m_bs[...] = (m_part[core, 1 - side].astype(F32) + m_a[1 - side].astype(F32)).astype(BF16)
            mix_b.start()

        @pl.when(at_step(i, 4))
        def _():
            d = i - 4
            s = chunk(d)
            give_b(d).wait_recv()
            total = part[s, core, side].astype(F32) + a_recv[s, side].astype(F32) + b_recv[s].astype(F32)

            @pl.when(d == 0)
            def _():
                c_recv[s] = total.astype(BF16)

            @pl.when(d > 0)
            def _():
                c_send[s] = total.astype(BF16)
                give_c(d).start()

    mix_b.wait_recv()
    mix_out[...] = (
        m_part[core, side].astype(F32) + m_a[side].astype(F32) + m_b[...].astype(F32)
    ).astype(BF16)

    @pl.loop(1, experts)
    def _(d):
        give_c_in(d).wait_recv()

    weight = wmat[...]
    high = weight.astype(BF16)
    low = (weight - high.astype(F32)).astype(BF16)
    tile = min(512, width)
    for n in range(0, width, tile):
        results = joined(c_recv[:, :, n : n + tile])
        moe_out[:, n : n + tile] = (
            jnp.dot(high, results, preferred_element_type=F32)
            + jnp.dot(low, results, preferred_element_type=F32)
        ).astype(BF16)

    mix_a.wait_send()
    mix_b.wait_send()

    @pl.loop(0, experts)
    def _(d):
        @pl.when(d > 0)
        def _():
            prim(d).wait_send()
            give_c(d).wait_send()

        xf(d).wait_send()
        cf(d).wait_send()
        cf2(d).wait_send()
        give_a(d).wait_send()
        give_b(d).wait_send()


def shards(
    conv_value,
    conv_gate,
    conv_kernel,
    norm_gain,
    mixer_proj,
    moe_in,
    route_ids,
    route_logits,
    moe_gain,
    expert_gate,
    expert_lin,
    expert_down,
):
    tp_size = lax.axis_size("tp")
    tp_index = lax.axis_index("tp")
    glu = (conv_value.astype(jnp.float32) * jax.nn.sigmoid(conv_gate.astype(jnp.float32))).astype(
        jnp.bfloat16
    )
    reach = conv_kernel.shape[0] - 1
    length = glu.shape[0]
    rim = passed_along(glu[length - reach :], "ep", 1)
    padded = jnp.concatenate([rim, glu], axis=0).astype(jnp.float32)
    conv = jnp.zeros(glu.shape, jnp.float32)
    for tap in range(reach + 1):
        conv = conv + conv_kernel[tap][None, :] * padded[tap : tap + length]
    total, square = lax.psum((jnp.sum(conv, axis=1), jnp.sum(conv * conv, axis=1)), "tp")
    channels = conv.shape[1] * tp_size
    mean = (total / channels)[:, None]
    var = (square / channels)[:, None] - mean * mean
    conv_act = jax.nn.silu((conv - mean) * lax.rsqrt(var + EPS) * norm_gain).astype(jnp.bfloat16)

    rows = moe_in.shape[0] // tp_size
    topk = route_ids.shape[1]
    experts = lax.axis_size("ep")
    capacity = max(2, 2 * rows * topk // experts)
    width = moe_in.shape[1]
    start = tp_index * rows
    block = lax.dynamic_slice_in_dim(moe_in, start, rows, 0).astype(jnp.float32)
    mu = jnp.mean(block, axis=1, keepdims=True)
    va = jnp.mean(jnp.square(block - mu), axis=1, keepdims=True)
    normed = ((block - mu) * lax.rsqrt(va + EPS) * moe_gain).astype(jnp.bfloat16)
    routes = lax.dynamic_slice_in_dim(route_ids, start, rows, 0)
    target = slot_targets(routes, experts, capacity).reshape(rows, topk)
    logits = lax.dynamic_slice_in_dim(route_logits, start, rows, 0)
    expo = jnp.exp(logits)
    weight = expo / jnp.sum(expo, axis=1, keepdims=True)
    slots = jnp.arange(experts * capacity, dtype=jnp.int32)
    hits = target[:, :, None] == slots[None, None, :]
    placed = jnp.any(hits, axis=1).astype(jnp.bfloat16)
    wmat = jnp.sum(jnp.where(hits, weight[:, :, None], 0.0), axis=1)
    packed = lax.dot_general(
        placed, normed, (((0,), (0,)), ((), ())), preferred_element_type=jnp.float32
    ).astype(jnp.bfloat16)
    packed = packed.reshape(experts, capacity, width)

    hid = expert_gate.shape[2]
    chans = conv_act.shape[1]
    vmem = pl.BlockSpec(memory_space=pltpu.VMEM)
    hbm = pl.BlockSpec(memory_space=pl.ANY)
    out = jax.ShapeDtypeStruct((rows, width), BF16)
    mixer_out, moe_out = pl.pallas_call(
        layer_kernel,
        out_shape=(out, out),
        in_specs=[vmem, vmem, vmem, hbm, hbm, hbm, hbm],
        out_specs=(vmem, vmem),
        scratch_shapes=[
            pltpu.VMEM((width, hid), BF16),
            pltpu.VMEM((width, hid), BF16),
            pltpu.VMEM((hid, width), BF16),
            pltpu.VMEM((chans, width), BF16),
            pltpu.VMEM((experts, tp_size, capacity, width), BF16),
            pltpu.VMEM((experts, 2, 2, capacity, width), BF16),
            pltpu.VMEM((experts, 2, capacity, width), BF16),
            pltpu.VMEM((experts, capacity, width), BF16),
            pltpu.VMEM((experts, capacity, width), BF16),
            pltpu.VMEM((experts, capacity, width), BF16),
            pltpu.VMEM((experts, capacity, width), BF16),
            pltpu.VMEM((2, 2, rows, width), BF16),
            pltpu.VMEM((2, rows, width), BF16),
            pltpu.VMEM((rows, width), BF16),
            pltpu.VMEM((rows, width), BF16),
            pltpu.SemaphoreType.DMA((5,)),
            pltpu.SemaphoreType.DMA((14, experts)),
            pltpu.SemaphoreType.DMA((4,)),
        ],
        compiler_params=pltpu.CompilerParams(
            has_side_effects=True, vmem_limit_bytes=60 * 1024 * 1024
        ),
    )(packed, conv_act, wmat, expert_gate[0], expert_lin[0], expert_down[0], mixer_proj)
    return (mixer_out, moe_out)


def solution(mesh):
    placed = (
        P("ep", "tp"),
        P("ep", "tp"),
        P(None, "tp"),
        P("tp"),
        P("tp", None),
        P("ep", None),
        P("ep", None),
        P("ep", None),
        P(),
        P("ep", None, "tp"),
        P("ep", None, "tp"),
        P("ep", "tp", None),
    )
    return jax.shard_map(
        shards,
        mesh=mesh,
        in_specs=placed,
        out_specs=(P(("ep", "tp"), None), P(("ep", "tp"), None)),
        check_vma=False,
    )
```

time: 297 us -> 180 us (0.61)
  waiting for transfers between devices: 156 us -> 0.01 us
  Pallas kernels: 0 us -> 146 us
  blocking collectives: 61.6 us -> 6.31 us
  matrix products: 24.5 us -> 2.19 us
  between operations: 14 us -> 0.79 us
  other arithmetic: 18.7 us -> 12.7 us
  local copies, waits for them, and re-layouts: 12.2 us -> 6.8 us
  starting transfers between devices: 9.16 us -> 4.9 us
    pallas_call x0 -> x1, Pallas kernels: none -> 146 us  [shards(): pl.pallas_call(layer_kernel, out_shape=(out, out), in_specs=[vmem, vmem,...]
    all_gather x1 -> x0, waiting for transfers between devices: 57.4 us -> none  [shards(): arrived = lax.all_gather(landed, 'tp', axis=0, tiled=True)]
    all_to_all x1 -> x0, blocking collectives: 55.4 us -> none  [shards(): lax.all_to_all(packed[None], 'ep', split_axis=1, concat_axis=1, tiled=True)]
    reduce_scatter x2 -> x0, waiting for transfers between devices: 49.3 us -> none  [the longest x1 49.3 us: shards(): lax.psum_scatter(jnp.dot(hidden, expert_down[0], preferred_element_type=j...]
    all_to_all x1 -> x0, waiting for transfers between devices: 47.7 us -> none  [shards(): lax.all_to_all(results.reshape(experts, capacity, width), 'ep', split_axi...]
    dot_general x4 -> x1, matrix products: 24.5 us -> 2.19 us  [shards(): lax.dot_general(placed, normed, (((0,), (0,)), ((), ())), preferred_eleme...]
    gather x2 -> x0, local copies, waits for them, and re-layouts: 7.57 us -> none  [the longest x1 4.22 us: shards(): returned.reshape(experts * capacity, width)[own_target].astype(jnp.float32)]
    all_to_all x1 -> x0, starting transfers between devices: 5.65 us -> none  [shards(): lax.all_to_all(results.reshape(experts, capacity, width), 'ep', split_axi...]
  transfers between devices with their start and end apart: 5 -> 1, of which waited for: 4 -> 0; matrix products, arithmetic and copies ran while one was open for 8% -> 5% of each run, Pallas kernels for 0% -> 0%
where the time goes in v1:
time: 180 us; the launch traced here: 179 us
  Pallas kernels  146 us (81%)
  other arithmetic  12.7 us (7%)
  local copies, waits for them, and re-layouts  6.8 us (4%)
  blocking collectives  6.31 us (4%)
  starting transfers between devices  4.9 us (3%)
  matrix products  2.19 us (1%)
    pallas_call x1, Pallas kernels, shards(): pl.pallas_call(layer_kernel, out_shape=(out, out), in_specs=[vmem, vmem,...  146 us
    psum x1, blocking collectives, shards(): lax.psum((jnp.sum(conv, axis=1), jnp.sum(conv * conv, axis=1)), 'tp')  6.31 us
    reduce_sum x1, other arithmetic, shards(): jnp.sum(conv, axis=1)  5.05 us
    ppermute x1, starting transfers between devices, passed_along(): return lax.ppermute(block, axis, route)  4.9 us
    unnamed x11, local copies, waits for them, and re-layouts  3.9 us
  transfers between devices with their start and end apart: 1, of which 0 were waited for; matrix products, arithmetic and copies ran while one was open for 5% of the time, Pallas kernels for 0%

profile of v1, /device:TPU:0, one launch (start us, length us, event | category | flops | bytes accessed | tf_op | source)
XLA Modules:
  0.0 179.3 jit_solution(3048502723861360594)
XLA Ops:
  0.6 0.0 copy-start
  0.6 0.0 copy-start.1
  0.7 0.0 copy-start.2
  0.7 1.6 multiply_convert_fusion.1
  2.3 4.9 %collective-permute-start = (bf16[30,512]{1,0:T(8,128)(2,1)S(1)}, bf16[30,512]{1,0:T(8,128)(2,1)S(1)}, u32[]{:S(2)}, u32[]{:S(2)}) collective-permute-start(bf16[30,512]{1,0:T(8,128)(2,1)S(1)} %slice.261), channel_id=1, source_target_pairs={{0,4},{4,8},{8,12},{12,16},{16,20},{20,24},{24,28},{1,5},{5,9},{9,... | collective-permute-start | bytes 92168 | tf_op jit(solution)/shard_map/ppermute | solution.py:18
  7.2 1.0 fusion.48
  8.3 1.2 fusion.47
  9.4 0.0 copy-done
  9.5 0.1 copy.20
  9.6 0.1 eq.42
  9.7 0.1 eq.38
  9.9 0.7 fusion.44
  10.6 0.7 broadcast_divide_fusion
  11.3 1.2 convert_reduce_fusion
  12.5 0.0 copy-done.1
  12.5 0.3 fusion.2
  12.8 0.6 reduce-window.6
  13.4 0.2 slice_reduce_fusion
  13.6 0.1 fusion.41
  13.7 0.1 sub.31
  13.9 0.1 copy.19
  13.9 0.1 fusion.39
  14.1 0.0 copy-done.2
  14.1 2.2 %convolution_convert_fusion = bf16[512,2048]{1,0:T(8,128)(2,1)} fusion(pred[128,512]{1,0:T(8,128)(4,1)S(1)} %fusion.39, f32[2048]{0:T(1024)S(1)} %copy-done.2, f32[128]{0:T(128)S(1)} %add_rsqrt_fusion.1, f32[128]{0:T(128)S(1)} %broadcast_multiply_fusion.1, bf16[512,2048]{1,0:T(8,128)(2,1)S(1)} %copy-done.1, s32[]{:T(128)S(6)} %select_n.9), kind=kOutput, calls=%fused_computation | convolution fusion | flops 270794752 | bytes 2696196 | tf_op jit(solution)/shard_map/dot_general | solution.py:295
  16.3 0.8 select_reduce_fusion.wmat
  17.1 0.0 collective-permute-done
  17.1 0.2 maximum_convert_fusion
  17.3 0.0 copy-start.3
  17.3 5.1 %fusion.45 = (f32[512]{0:T(512)S(1)}, f32[512]{0:T(512)S(1)}, f32[512,512]{1,0:T(8,128)S(1)}) fusion(f32[542,512]{1,0:T(8,128)S(1)} %maximum_convert_fusion, f32[512]{0:T(512)S(1)} %bitcast.56, f32[512]{0:T(512)S(1)} %bitcast.57, f32[512]{0:T(512)S(1)} %bitcast.59, f32[512]{0:T(512)S(1)} %bitcast.60, f32[512]{0:T(512)S(1)} %bitcast.61, f32[512]{0:T(512)S(1)} %bitcast.62, ...), kind=kLoop, calls=%fused_computation.97 | loop fusion | flops 16776192 | bytes 33622016 | tf_op jit(solution)/shard_map/reduce_sum | solution.py:270
  22.4 6.3 %all-reduce = (f32[512]{0:T(512)S(1)}, f32[512]{0:T(512)S(1)}) all-reduce(f32[512]{0:T(512)S(1)} %get-tuple-element.3, f32[512]{0:T(512)S(1)} %get-tuple-element.2), channel_id=1, replica_groups=mesh['ep'=8,'tp'=4] {'tp'}, use_global_device_ids=true, to_apply=%region_9.10 | all-reduce | flops 1024 | bytes 8192 | tf_op jit(solution)/shard_map/psum | solution.py:270
  28.7 0.0 copy-done.3
  28.7 1.2 multiply_convert_fusion.act
  29.9 145.7 %shard_map.131 = (bf16[128,2048]{1,0:T(8,128)(2,1)}, bf16[128,2048]{1,0:T(8,128)(2,1)}) custom-call(bf16[8,64,2048]{2,1,0:T(8,128)(2,1)} %bitcast.42, bf16[512,512]{1,0:T(8,128)(2,1)} %multiply_convert_fusion.act, f32[128,512]{1,0:T(8,128)} %select_reduce_fusion.wmat, bf16[2048,512]{1,0:T(8,128)(2,1)} %bitcast.43, bf16[2048,512]{1,0:T(8,128)(2,1)} %bitcast.44, ...), custom_call_target="tpu_custom_call" | custom-call | tf_op jit(solution)/shard_map/pallas_call | solution.py:305
  175.6 1.9 %copy.23 = bf16[128,2048]{1,0:T(8,128)(2,1)} copy(bf16[128,2048]{1,0:T(8,128)(2,1)} %get-tuple-element.42) | data formatting | bytes 1048576
  177.4 1.9 %copy.24 = bf16[128,2048]{1,0:T(8,128)(2,1)} copy(bf16[128,2048]{1,0:T(8,128)(2,1)} %get-tuple-element.43) | data formatting | bytes 1048576
  (10 shorter events, 0.1 us)
Async XLA Ops:
  0.6 8.8 %copy-start = (s32[512,2]{0,1:T(2,128)S(1)}, s32[512,2]{0,1:T(2,128)}, u32[]{:S(2)}) copy-start(s32[512,2]{0,1:T(2,128)} %param.18) | copy-start | bytes 12292
  0.6 11.8 %copy-start.1 = (bf16[512,2048]{1,0:T(8,128)(2,1)S(1)}, bf16[512,2048]{1,0:T(8,128)(2,1)}, u32[]{:S(2)}) copy-start(bf16[512,2048]{1,0:T(8,128)(2,1)} %param.17) | copy-start | bytes 6291460
  0.7 13.4 %copy-start.2 = (f32[2048]{0:T(1024)S(1)}, f32[2048]{0:T(1024)}, u32[]{:S(2)}) copy-start(f32[2048]{0:T(1024)} %param.20) | copy-start | bytes 24580
  2.3 14.8 %collective-permute-start = (bf16[30,512]{1,0:T(8,128)(2,1)S(1)}, bf16[30,512]{1,0:T(8,128)(2,1)S(1)}, u32[]{:S(2)}, u32[]{:S(2)}) collective-permute-start(bf16[30,512]{1,0:T(8,128)(2,1)S(1)} %slice.261), channel_id=1, source_target_pairs={{0,4},{4,8},{8,12},{12,16},{16,20},{20,24},{24,28},{1,5},{5,9},{9,... | collective-permute-start | bytes 92168 | tf_op jit(solution)/shard_map/ppermute | solution.py:18
  17.3 11.4 %copy-start.3 = (f32[512]{0:T(512)S(1)}, f32[512]{0:T(512)}, u32[]{:S(2)}) copy-start(f32[512]{0:T(512)} %param.15) | copy-start | bytes 6148

commit v2 on v1

--- a/solution.py
+++ b/solution.py
@@ -10,12 +10,6 @@
 SLOPE = 1.702
 F32 = jnp.float32
 BF16 = jnp.bfloat16
-
-
-def passed_along(block, axis, distance):
-    devices = range(lax.axis_size(axis))
-    route = [(i - distance, i) for i in devices if i - distance in devices]
-    return lax.ppermute(block, axis, route)
 
 
 def slot_targets(routes, experts, capacity):
@@ -44,11 +38,12 @@
 
 
 def layer_kernel(
-    packed, act, wmat, gate_hbm, lin_hbm, down_hbm, proj_hbm,
+    packed, wmat, value, gates, taps, gain, gate_hbm, lin_hbm, down_hbm, proj_hbm,
     mix_out, moe_out,
     gate_w, lin_w, down_w, proj_w,
     arrived, part, a_recv, b_send, b_recv, c_send, c_recv,
     m_part, m_a, m_bs, m_b,
+    glu, halo, padded, conv, s_own, s_core, s_pair, s_side,
     load_sem, sems, m_sems,
 ):
     experts, cap, width = packed.shape
@@ -112,6 +107,70 @@
 
     mix_a = remote(m_part.at[1 - core], m_a, m_sems.at[0], m_sems.at[1], cpeer)
     mix_b = remote(m_bs, m_b, m_sems.at[2], m_sems.at[3], xpeer)
+
+    length, rim = glu.shape[0], halo.shape[0]
+    reach = taps.shape[0] - 1
+    channels = glu.shape[1] * 4
+    forward = lax.rem(ep + 1, experts)
+    edge = remote(glu.at[pl.ds(length - rim, rim)], halo, m_sems.at[4], m_sems.at[5], {"ep": forward})
+    stat_a = remote(s_own, s_core, m_sems.at[6], m_sems.at[7], cpeer)
+    stat_b = remote(s_pair, s_side, m_sems.at[8], m_sems.at[9], xpeer)
+
+    def gated():
+        glu[...] = (value[...].astype(F32) * jax.nn.sigmoid(gates[...].astype(F32))).astype(BF16)
+
+        @pl.when(ep < experts - 1)
+        def _():
+            edge.start()
+
+        padded[rim:, :] = glu[...].astype(F32)
+
+    def convolved():
+        @pl.when(ep > 0)
+        def _():
+            edge.wait_recv()
+            padded[:rim, :] = halo[...].astype(F32)
+
+        @pl.when(ep == 0)
+        def _():
+            padded[:rim, :] = jnp.zeros((rim, padded.shape[1]), F32)
+
+        step = min(64, length)
+
+        @pl.loop(0, glu.shape[1] // 128)
+        def _(j):
+            lanes = pl.ds(pl.multiple_of(j * 128, 128), 128)
+            for r in range(0, length, step):
+                total = jnp.zeros((step, 128), F32)
+                for tap in range(reach + 1):
+                    first = r + rim - reach + tap
+                    total = total + taps[tap : tap + 1, lanes] * padded[first : first + step, lanes]
+                conv[r : r + step, lanes] = total
+
+        full = conv[...]
+        lane = lax.broadcasted_iota(jnp.int32, s_own.shape, 1)
+        s_own[...] = jnp.where(
+            lane == 0,
+            jnp.sum(full, axis=1, keepdims=True),
+            jnp.where(lane == 1, jnp.sum(full * full, axis=1, keepdims=True), 0.0),
+        )
+        stat_a.start()
+
+    def paired():
+        stat_a.wait_recv()
+        s_pair[...] = s_own[...] + s_core[...]
+        stat_b.start()
+
+    def projected():
+        stat_b.wait_recv()
+        for t in range(4):
+            own_rows = slice(t * rows, (t + 1) * rows)
+            stats = s_pair[own_rows, :] + s_side[own_rows, :]
+            mean = stats[:, 0:1] / channels
+            var = stats[:, 1:2] / channels - mean * mean
+            act = jax.nn.silu((conv[own_rows, :] - mean) * lax.rsqrt(var + EPS) * gain[...]).astype(BF16)
+            m_part[t % 2, t // 2] = jnp.dot(act, proj_w[...], preferred_element_type=F32).astype(BF16)
+        mix_a.start()
 
     own.start()
 
@@ -131,13 +190,8 @@
     xf(0).start()
     cf(0).start()
 
-    loads[0].wait()
-    for t in range(4):
-        m_part[t % 2, t // 2] = jnp.dot(
-            act[t * rows : (t + 1) * rows, :], proj_w[...], preferred_element_type=F32
-        ).astype(BF16)
-    mix_a.start()
-    for load in loads[1:]:
+    gated()
+    for load in loads:
         load.wait()
 
     def ffn(d):
@@ -182,7 +236,19 @@
             b_send[s] = (part[s, core, 1 - side].astype(F32) + a_recv[s, 1 - side].astype(F32)).astype(BF16)
             give_b(d).start()
 
+        @pl.when(i == 1)
+        def _():
+            convolved()
+
+        @pl.when(i == 2)
+        def _():
+            paired()
+
         @pl.when(i == 3)
+        def _():
+            projected()
+
+        @pl.when(i == 4)
         def _():
             mix_a.wait_recv()
             m_bs[...] = (m_part[core, 1 - side].astype(F32) + m_a[1 - side].astype(F32)).astype(BF16)
@@ -224,6 +290,12 @@
             + jnp.dot(low, results, preferred_element_type=F32)
         ).astype(BF16)
 
+    @pl.when(ep < experts - 1)
+    def _():
+        edge.wait_send()
+
+    stat_a.wait_send()
+    stat_b.wait_send()
     mix_a.wait_send()
     mix_b.wait_send()
 
@@ -257,22 +329,6 @@
 ):
     tp_size = lax.axis_size("tp")
     tp_index = lax.axis_index("tp")
-    glu = (conv_value.astype(jnp.float32) * jax.nn.sigmoid(conv_gate.astype(jnp.float32))).astype(
-        jnp.bfloat16
-    )
-    reach = conv_kernel.shape[0] - 1
-    length = glu.shape[0]
-    rim = passed_along(glu[length - reach :], "ep", 1)
-    padded = jnp.concatenate([rim, glu], axis=0).astype(jnp.float32)
-    conv = jnp.zeros(glu.shape, jnp.float32)
-    for tap in range(reach + 1):
-        conv = conv + conv_kernel[tap][None, :] * padded[tap : tap + length]
-    total, square = lax.psum((jnp.sum(conv, axis=1), jnp.sum(conv * conv, axis=1)), "tp")
-    channels = conv.shape[1] * tp_size
-    mean = (total / channels)[:, None]
-    var = (square / channels)[:, None] - mean * mean
-    conv_act = jax.nn.silu((conv - mean) * lax.rsqrt(var + EPS) * norm_gain).astype(jnp.bfloat16)
-
     rows = moe_in.shape[0] // tp_size
     topk = route_ids.shape[1]
     experts = lax.axis_size("ep")
@@ -298,14 +354,15 @@
     packed = packed.reshape(experts, capacity, width)
 
     hid = expert_gate.shape[2]
-    chans = conv_act.shape[1]
+    length, chans = conv_value.shape
+    rim = -(-(conv_kernel.shape[0] - 1) // 16) * 16
     vmem = pl.BlockSpec(memory_space=pltpu.VMEM)
     hbm = pl.BlockSpec(memory_space=pl.ANY)
     out = jax.ShapeDtypeStruct((rows, width), BF16)
     mixer_out, moe_out = pl.pallas_call(
         layer_kernel,
         out_shape=(out, out),
-        in_specs=[vmem, vmem, vmem, hbm, hbm, hbm, hbm],
+        in_specs=[vmem] * 6 + [hbm, hbm, hbm, hbm],
         out_specs=(vmem, vmem),
         scratch_shapes=[
             pltpu.VMEM((width, hid), BF16),
@@ -323,14 +380,25 @@
             pltpu.VMEM((2, rows, width), BF16),
             pltpu.VMEM((rows, width), BF16),
             pltpu.VMEM((rows, width), BF16),
+            pltpu.VMEM((length, chans), BF16),
+            pltpu.VMEM((rim, chans), BF16),
+            pltpu.VMEM((rim + length, chans), F32),
+            pltpu.VMEM((length, chans), F32),
+            pltpu.VMEM((length, 128), F32),
+            pltpu.VMEM((length, 128), F32),
+            pltpu.VMEM((length, 128), F32),
+            pltpu.VMEM((length, 128), F32),
             pltpu.SemaphoreType.DMA((5,)),
             pltpu.SemaphoreType.DMA((14, experts)),
-            pltpu.SemaphoreType.DMA((4,)),
+            pltpu.SemaphoreType.DMA((10,)),
         ],
         compiler_params=pltpu.CompilerParams(
             has_side_effects=True, vmem_limit_bytes=60 * 1024 * 1024
         ),
-    )(packed, conv_act, wmat, expert_gate[0], expert_lin[0], expert_down[0], mixer_proj)
+    )(
+        packed, wmat, conv_value, conv_gate, conv_kernel, norm_gain[None, :],
+        expert_gate[0], expert_lin[0], expert_down[0], mixer_proj,
+    )
     return (mixer_out, moe_out)
 
 

time: 180 us -> 182 us (1.011)
  the two profiles are of different devices: /device:TPU:0 before, /device:TPU:20 now
where the time goes in v2:
time: 182 us
  Pallas kernels  167 us (92%)
  other arithmetic  5.65 us (3%)
  local copies, waits for them, and re-layouts  4.59 us (3%)
  matrix products  3.24 us (2%)
    pallas_call x1, Pallas kernels, shards(): pl.pallas_call(layer_kernel, out_shape=(out, out), in_specs=[vmem] * 6 +...  167 us
    unnamed x5, local copies, waits for them, and re-layouts  3.88 us

profile of v2, /device:TPU:20, one launch (start us, length us, event | category | flops | bytes accessed | tf_op | source)
XLA Modules:
  0.0 181.5 jit_solution(5614969914847119844)
XLA Ops:
  0.6 0.0 copy-start
  0.6 0.7 fusion.14
  1.3 0.7 broadcast_divide_fusion
  2.0 1.2 convert_reduce_fusion
  3.2 1.3 fusion.2
  4.6 0.0 copy-done
  4.6 0.1 copy.20
  4.7 0.1 eq.42
  4.9 0.1 eq.38
  5.0 0.6 reduce-window.6
  5.6 0.2 slice_reduce_fusion
  5.9 0.1 fusion.11
  6.0 0.1 sub.9
  6.1 0.1 copy.19
  6.2 0.1 fusion.9
  6.3 0.8 select_reduce_fusion.wmat
  7.2 3.2 %convolution_convert_fusion = bf16[512,2048]{1,0:T(8,128)(2,1)} fusion(pred[128,512]{1,0:T(8,128)(4,1)S(1)} %fusion.9, f32[2048]{0:T(1024)} %param.20, f32[128]{0:T(128)S(1)} %add_rsqrt_fusion, f32[128]{0:T(128)S(1)} %broadcast_multiply_fusion, bf16[512,2048]{1,0:T(8,128)(2,1)} %param.17, s32[]{:T(128)S(6)} %select_n.9), kind=kOutput, calls=%fused_computation | convolution fusion | flops 270794752 | bytes 2696196 | tf_op jit(solution)/shard_map/dot_general | solution.py:351
  10.4 167.3 %shard_map.131 = (bf16[128,2048]{1,0:T(8,128)(2,1)}, bf16[128,2048]{1,0:T(8,128)(2,1)}) custom-call(bf16[8,64,2048]{2,1,0:T(8,128)(2,1)} %bitcast.12, f32[128,512]{1,0:T(8,128)} %select_reduce_fusion.wmat, bf16[512,512]{1,0:T(8,128)(2,1)} %value.1, bf16[512,512]{1,0:T(8,128)(2,1)} %gates.1, f32[31,512]{1,0:T(8,128)} %taps.1, f32[1,512]{1,0:T(1,128)} %bitcast.16, ...), custom_call_target="tpu_custom_call" | custom-call | tf_op jit(solution)/shard_map/pallas_call | solution.py:362
  177.8 1.9 %copy.23 = bf16[128,2048]{1,0:T(8,128)(2,1)} copy(bf16[128,2048]{1,0:T(8,128)(2,1)} %get-tuple-element.4) | data formatting | bytes 1048576
  179.6 1.9 %copy.24 = bf16[128,2048]{1,0:T(8,128)(2,1)} copy(bf16[128,2048]{1,0:T(8,128)(2,1)} %get-tuple-element.5) | data formatting | bytes 1048576
  (8 shorter events, 0.1 us)
Async XLA Ops:
  0.6 4.0 %copy-start = (s32[512,2]{0,1:T(2,128)S(1)}, s32[512,2]{0,1:T(2,128)}, u32[]{:S(2)}) copy-start(s32[512,2]{0,1:T(2,128)} %param.18) | copy-start | bytes 12292
